TPU v7x, 32 devices: a whole 2x2x4 slice. The times are simulated.
32 devices in a mesh: rep: 2 (over core), fs: 8 (over z, y), tp: 2 (over x).
Axes of the slice: x: 2, y: 2, z: 4, core: 2. Of those that a mesh axis runs over, the one named last changes fastest.
Arguments:
- tokens: bfloat16 [16, 768, 2048], P(('rep', 'fs')), may hold values from -6 to 6
- mixer_gain: float32 [2048], replicated, may hold values from 0.1 to 1.9
- value_weight: float32 [2048, 4, 512], P('fs', None, 'tp'), may hold values from -0.125 to 0.125
- value_scale: float32 [4, 512], P(None, 'tp'), may hold values from 0.5 to 2
- gate_weight: float32 [2048, 4, 512], P('fs', None, 'tp'), may hold values from -0.125 to 0.125
- gate_scale: float32 [4, 512], P(None, 'tp'), may hold values from 0.5 to 2
- pool_weight: float32 [4, 512, 512], P(None, 'fs', 'tp'), may hold values from -0.25 to 0.25
- pool_scale: float32 [4, 512], P(None, 'tp'), may hold values from 0.5 to 2
- channel_gain: float32 [2048], replicated, may hold values from 0.1 to 1.9
- up_weight: float32 [2048, 4096], P('fs', 'tp'), may hold values from -0.125 to 0.125
- up_scale: float32 [4096], P('tp'), may hold values from 0.5 to 2
- down_weight: float32 [4096, 2048], P('tp', 'fs'), may hold values from -0.09375 to 0.09375
- down_scale: float32 [2048], P('fs'), may hold values from 0.5 to 2
Outputs:
- layer_out: bfloat16 [16, 768, 2048], P(('rep', 'fs'), 'tp')
All inputs are finite; a program needn't handle non-finite values.
Results may differ from a plain program's by a relative error of at most 0.015.
Values may be sent and summed in bfloat16 or wider, within the bound.
A program may use at most 64 MiB of HBM per device.

v0:
```python
import jax
import jax.numpy as jnp
from jax import lax
from jax.sharding import PartitionSpec as P


def norm_rows(values, gain):
    floats = values.astype(jnp.float32)
    return floats * lax.rsqrt(jnp.mean(floats * floats, axis=-1, keepdims=True) + 1e-06) * gain


def pool_excess(value):
    floats = value.astype(jnp.float32)
    seq_length = floats.shape[1]
    running = floats
    results = []
    for group in range(floats.shape[2]):
        span = 2**group
        shifted = jnp.pad(running, ((0, 0), (span, 0), (0, 0), (0, 0)))[:, :seq_length]
        running = running + shifted
        counts = jnp.minimum(jnp.arange(1, seq_length + 1), 2 * span).astype(jnp.float32)
        results.append(running[:, :, group, :] / counts[None, :, None] - floats[:, :, group, :])
    return jnp.stack(results, axis=2)


def per_device(
    tokens,
    mixer_gain,
    value_weight,
    value_scale,
    gate_weight,
    gate_scale,
    pool_weight,
    pool_scale,
    channel_gain,
    up_weight,
    up_scale,
    down_weight,
    down_scale,
):
    seq_count, seq_length, model_width = tokens.shape
    shares = lax.axis_size("tp")
    member = lax.axis_index("tp")
    kept_rows = seq_length // shares
    row_count = seq_count * seq_length
    group_count, local_width = value_scale.shape
    value_full, gate_full, pool_full = (
        lax.all_gather(value_weight.astype(jnp.bfloat16), "fs", axis=0, tiled=True),
        lax.all_gather(gate_weight.astype(jnp.bfloat16), "fs", axis=0, tiled=True),
        lax.all_gather(pool_weight.astype(jnp.bfloat16), "fs", axis=1, tiled=True),
    )
    down_scales = lax.all_gather(down_scale, "fs", axis=0, tiled=True)
    normed = norm_rows(tokens, mixer_gain).astype(jnp.bfloat16).reshape(row_count, model_width)
    value = jnp.dot(normed, value_full.reshape(model_width, -1), preferred_element_type=jnp.float32)
    value = (
        (value * value_scale.reshape(-1))
        .astype(jnp.bfloat16)
        .reshape(seq_count, seq_length, group_count, local_width)
    )
    gating = jnp.dot(normed, gate_full.reshape(model_width, -1), preferred_element_type=jnp.float32)
    gating = (gating * gate_scale.reshape(-1)).reshape(
        seq_count, seq_length, group_count, local_width
    )
    excess = pool_excess(value).astype(jnp.bfloat16)
    rows_part = pool_full
    pooled = jnp.einsum(
        "slgc,gce->slge",
        lax.all_gather(excess, "tp", axis=3, tiled=True),
        rows_part,
        preferred_element_type=jnp.float32,
    )
    merged = (jax.nn.sigmoid(gating) * (pooled * pool_scale)).astype(jnp.bfloat16)
    merged_own = lax.all_to_all(merged, "tp", split_axis=1, concat_axis=3, tiled=True)
    own_rows = lax.dynamic_slice_in_dim(tokens, member * kept_rows, kept_rows, 1)
    middle = own_rows.reshape(seq_count * kept_rows, model_width).astype(
        jnp.float32
    ) + merged_own.reshape(seq_count * kept_rows, model_width).astype(jnp.float32)
    normed_two = norm_rows(middle, channel_gain).astype(jnp.bfloat16)
    up_full, down_full = (
        lax.all_gather(up_weight.astype(jnp.bfloat16), "fs", axis=0, tiled=True),
        lax.all_gather(down_weight.astype(jnp.bfloat16), "fs", axis=1, tiled=True),
    )
    upward = (
        jnp.dot(
            lax.all_gather(normed_two, "tp", axis=0, tiled=True),
            up_full,
            preferred_element_type=jnp.float32,
        )
        * up_scale
    )
    hidden = jnp.square(jax.nn.relu(upward)).astype(jnp.bfloat16)
    rows_part = hidden
    summed = lax.psum_scatter(
        (jnp.dot(rows_part, down_full, preferred_element_type=jnp.float32) * down_scales).astype(
            jnp.bfloat16
        ),
        "tp",
        scatter_dimension=0,
        tiled=True,
    ).astype(jnp.float32)
    return (middle + summed).astype(jnp.bfloat16).reshape(seq_count, kept_rows, model_width)


def solution(mesh):
    return jax.shard_map(
        per_device,
        mesh=mesh,
        in_specs=(
            P(("rep", "fs"), None, None),
            P(),
            P("fs", None, "tp"),
            P(None, "tp"),
            P("fs", None, "tp"),
            P(None, "tp"),
            P(None, "fs", "tp"),
            P(None, "tp"),
            P(),
            P("fs", "tp"),
            P("tp"),
            P("tp", "fs"),
            P("fs"),
        ),
        out_specs=P(("rep", "fs"), "tp", None),
        check_vma=False,
    )
```

profile of v0, /device:TPU:0, one launch (start us, length us, event | category | flops | bytes accessed | tf_op | source)
XLA Modules:
  0.0 646.4 jit_solution(14735097073703122514)
XLA Ops:
  6.5 2.3 convert_element_type.124
  9.0 2.2 convert_element_type.123
  12.8 72.2 %all-gather.11.cloned.1.call-done = bf16[2048,4,256]{2,1,0:T(4,128)(2,1)} async-done(((bf16[256,4,256]{2,1,0:T(4,128)(2,1)}), bf16[2048,4,256]{2,1,0:T(4,128)(2,1)}) %all-gather.11.cloned.1.call-update) | async-done | bytes 4194320 | tf_op jit(solution)/shard_map/all_gather | solution.py:48
  85.0 3.2 copy.33
  88.3 5.2 fusion.12
  93.5 5.2 reshape.227
  98.6 2.5 copy.23
  103.3 1.3 pad_maximum_fusion
  104.7 53.8 %all-gather.9.cloned.1.call-done = bf16[2048,4,256]{2,1,0:T(4,128)(2,1)} async-done(((bf16[256,4,256]{2,1,0:T(4,128)(2,1)}), bf16[2048,4,256]{2,1,0:T(4,128)(2,1)}) %all-gather.9.cloned.1.call-update) | async-done | bytes 4194320 | tf_op jit(solution)/shard_map/all_gather | solution.py:49
  158.5 3.2 copy.31
  161.7 5.5 add_divide_fusion
  167.2 3.5 div.73
  170.7 28.8 %all-gather.15.cloned.1.call-done = bf16[4,512,256]{2,1,0:T(8,128)(2,1)} async-done(((bf16[4,64,256]{2,1,0:T(8,128)(2,1)}), bf16[4,512,256]{2,1,0:T(8,128)(2,1)}) %all-gather.15.cloned.1.call-update) | async-done | bytes 1048592 | tf_op jit(solution)/shard_map/all_gather | solution.py:50
  199.5 45.0 %all-gather.13.cloned.1.call-done = bf16[1,768,4,512]{3,1,2,0:T(8,128)(2,1)} async-done(((bf16[1,768,4,256]{3,1,2,0:T(8,128)(2,1)}), bf16[1,768,4,512]{3,1,2,0:T(8,128)(2,1)}) %all-gather.13.cloned.1.call-update) | async-done | bytes 3145744 | tf_op jit(solution)/shard_map/all_gather | solution.py:68
  244.5 3.3 fusion.9
  247.8 2.4 copy.29
  250.2 3.7 all-to-all-start
  254.1 19.0 %all-to-all-done = bf16[1,768,4,256]{3,2,0,1:T(4,128)(2,1)S(1)} async-done(((bf16[1,768,4,256]{3,2,0,1:T(4,128)(2,1)}), bf16[1,768,4,256]{3,2,0,1:T(4,128)(2,1)S(1)}, u32[]{:S(2)}, u32[]{:S(2)}) %all-to-all-start) | async-done | bytes 1572896 | tf_op jit(solution)/shard_map/all_to_all | solution.py:73
  273.1 4.1 copy.37
  277.2 4.1 reshape.228
  281.4 2.1 multiply_reduce_fusion
  283.7 1.6 multiply_convert_fusion.2
  285.4 2.7 convert_element_type.139
  288.2 2.6 convert_element_type.141
  290.9 20.5 %all-gather = f32[8,1,256]{2,1,0:T(1,128)S(1)} all-gather(f32[1,1,256]{2,1,0:T(1,128)S(1)} %bitcast.69), channel_id=1, replica_groups=mesh['rep'=2,'fs'=8,'tp'=2] {'fs'}, dimensions={0}, use_global_device_ids=true | all-gather | bytes 9216 | tf_op jit(solution)/shard_map/all_gather | solution.py:52
  311.5 19.0 %all-gather.17.cloned.1.call-done = bf16[768,2048]{1,0:T(8,128)(2,1)} async-done(((bf16[384,2048]{1,0:T(8,128)(2,1)}), bf16[768,2048]{1,0:T(8,128)(2,1)}) %all-gather.17.cloned.1.call-update) | async-done | bytes 3145744 | tf_op jit(solution)/shard_map/all_gather | solution.py:85
  330.4 126.5 %all-gather.19.cloned.1.call-done = bf16[2048,2048]{1,0:T(8,128)(2,1)} async-done(((bf16[256,2048]{1,0:T(8,128)(2,1)}), bf16[2048,2048]{1,0:T(8,128)(2,1)}) %all-gather.19.cloned.1.call-update) | async-done | bytes 8388624 | tf_op jit(solution)/shard_map/all_gather | solution.py:80
  456.9 11.9 %multiply_convert_fusion.1 = bf16[768,2048]{1,0:T(8,128)(2,1)} fusion(bf16[768,2048]{1,0:T(8,128)(2,1)} %all-gather.17.cloned.1.call-done, bf16[2048,2048]{1,0:T(8,128)(2,1)} %all-gather.19.cloned.1.call-done, f32[2048]{0:T(1024)S(1)} %copy-done.9), kind=kOutput, calls=%fused_computation.6 | convolution fusion | flops 6448742400 | bytes 14688256 | tf_op jit(solution)/shard_map/dot_general | solution.py:84
  468.9 113.2 %all-gather.21.cloned.1.call-done = bf16[2048,2048]{1,0:T(8,128)(2,1)} async-done(((bf16[2048,256]{1,0:T(8,128)(2,1)}), bf16[2048,2048]{1,0:T(8,128)(2,1)}) %all-gather.21.cloned.1.call-update) | async-done | bytes 8388624 | tf_op jit(solution)/shard_map/all_gather | solution.py:81
  582.1 11.9 %multiply_convert_fusion = bf16[768,2048]{1,0:T(8,128)(2,1)} fusion(bf16[768,2048]{1,0:T(8,128)(2,1)} %multiply_convert_fusion.1, bf16[2048,2048]{1,0:T(8,128)(2,1)} %all-gather.21.cloned.1.call-done, f32[2048]{0:T(1024)S(1)} %bitcast.64), kind=kOutput, calls=%fused_computation.5 | convolution fusion | flops 6445596672 | bytes 14688256 | tf_op jit(solution)/shard_map/dot_general | solution.py:94
  594.0 41.8 %reduce-scatter.2.cloned.1.call-done = bf16[384,2048]{1,0:T(8,128)(2,1)} async-done(((bf16[768,2048]{1,0:T(8,128)(2,1)}), bf16[384,2048]{1,0:T(8,128)(2,1)}) %reduce-scatter.2.cloned.1.call-update) | async-done | bytes 1572880 | tf_op jit(solution)/shard_map/reduce_scatter | solution.py:93
  635.8 3.8 fusion.15
  (49 shorter events, 4.5 us)
Async XLA Ops:
  6.5 4.7 copy-start.2
  6.5 5.5 copy-start
  6.5 78.5 %all-gather.11.cloned.1.call-start = ((), (), s32[]{:S(2)}) async-start(), calls=%async_computation.3 | async-start | bytes 4718592 | tf_op jit(solution)/shard_map/all_gather | solution.py:48
  8.9 3.9 copy-start.5
  8.9 149.6 %all-gather.9.cloned.1.call-start = ((), (), s32[]{:S(2)}) async-start(), calls=%async_computation.2 | async-start | bytes 4718592 | tf_op jit(solution)/shard_map/all_gather | solution.py:49
  11.2 188.3 %all-gather.15.cloned.1.call-start = ((), (), s32[]{:S(2)}) async-start(), calls=%async_computation.5 | async-start | bytes 1179648 | tf_op jit(solution)/shard_map/all_gather | solution.py:50
  12.0 232.5 %all-gather.13.cloned.1.call-start = ((), (), s32[]{:S(2)}) async-start(), calls=%async_computation.4 | async-start | bytes 4718592 | tf_op jit(solution)/shard_map/all_gather | solution.py:68
  85.0 3.2 copy-start.8
  103.3 1.4 copy-start.6
  167.2 77.3 %copy-start.3 = (f32[4,256]{1,0:T(4,128)S(1)}, f32[4,256]{1,0:T(4,128)}, u32[]{:S(2)}) copy-start(f32[4,256]{1,0:T(4,128)} %param.20) | copy-start | bytes 12292
  250.2 23.0 %all-to-all-start = ((bf16[1,768,4,256]{3,2,0,1:T(4,128)(2,1)}), bf16[1,768,4,256]{3,2,0,1:T(4,128)(2,1)S(1)}, u32[]{:S(2)}, u32[]{:S(2)}) async-start(bf16[1,768,4,256]{3,2,0,1:T(4,128)(2,1)} %copy.29), calls=%async_computation | async-start | bytes 3145728 | tf_op jit(solution)/shard_map/all_to_all | solution.py:73
  253.8 76.6 %all-gather.17.cloned.1.call-start = ((), (), s32[]{:S(2)}) async-start(), calls=%async_computation.6 | async-start | bytes 4718592 | tf_op jit(solution)/shard_map/all_gather | solution.py:85
  281.4 2.4 copy-start.1
  281.4 2.4 copy-start.4
  285.4 171.6 %all-gather.19.cloned.1.call-start = ((), (), s32[]{:S(2)}) async-start(), calls=%async_computation.7 | async-start | bytes 9437184 | tf_op jit(solution)/shard_map/all_gather | solution.py:80
  288.1 2.8 copy-start.7
  288.1 168.8 %copy-start.9 = (f32[2048]{0:T(1024)S(1)}, f32[2048]{0:T(1024)}, u32[]{:S(2)}) copy-start(f32[2048]{0:T(1024)} %param.23) | copy-start | bytes 24580
  288.2 294.0 %all-gather.21.cloned.1.call-start = ((), (), s32[]{:S(2)}) async-start(), calls=%async_computation.8 | async-start | bytes 9437184 | tf_op jit(solution)/shard_map/all_gather | solution.py:81
  290.9 344.9 %reduce-scatter.2.cloned.1.call-start = ((), (), s32[]{:S(2)}) async-start(), calls=%async_computation.9 | async-start | bytes 4718592 | tf_op jit(solution)/shard_map/reduce_scatter | solution.py:93
Sparse Core Ops, SparseCore 0:
  9.5 75.5 all-gather.10
  87.1 71.3 all-gather.8
  160.7 38.7 all-gather.14
  200.9 43.5 all-gather.12
  285.5 44.8 all-gather.16
  332.4 124.4 all-gather.18
  459.0 123.1 all-gather.20
  594.1 41.6 reduce-scatter.1
where the time goes:
time: 647 us; the launch traced here: 646 us
  waiting for transfers between devices  519 us (80%)
  matrix products  37.8 us (6%)
  local copies, waits for them, and re-layouts  28.8 us (4%)
  other arithmetic  21.9 us (3%)
  blocking collectives  20.5 us (3%)
  between operations  13.7 us (2%)
    all_gather x1, waiting for transfers between devices, per_device(): lax.all_gather(up_weight.astype(jnp.bfloat16), 'fs', axis=0, tiled=True)  126 us
    all_gather x1, waiting for transfers between devices, per_device(): lax.all_gather(down_weight.astype(jnp.bfloat16), 'fs', axis=1, tiled=True)  113 us
    all_gather x1, waiting for transfers between devices, per_device(): lax.all_gather(value_weight.astype(jnp.bfloat16), 'fs', axis=0, tiled=True)  72.2 us
    all_gather x1, waiting for transfers between devices, per_device(): lax.all_gather(gate_weight.astype(jnp.bfloat16), 'fs', axis=0, tiled=True)  53.8 us
    all_gather x1, waiting for transfers between devices, per_device(): lax.all_gather(excess, 'tp', axis=3, tiled=True)  45 us
    reduce_scatter x1, waiting for transfers between devices, per_device(): lax.psum_scatter((jnp.dot(rows_part, down_full, preferred_element_type=jn...  41.8 us
    all_gather x1, waiting for transfers between devices, per_device(): lax.all_gather(pool_weight.astype(jnp.bfloat16), 'fs', axis=1, tiled=True)  28.8 us
    all_gather x1, blocking collectives, per_device(): down_scales = lax.all_gather(down_scale, 'fs', axis=0, tiled=True)  20.5 us
  transfers between devices with their start and end apart: 9, of which 9 were waited for; matrix products, arithmetic and copies ran while one was open for 8% of the time, Pallas kernels for 0%

commit v1 on v0

--- a/solution.py
+++ b/solution.py
@@ -1,7 +1,170 @@
+import functools
+
 import jax
 import jax.numpy as jnp
 from jax import lax
+from jax.experimental import pallas as pl
+from jax.experimental.pallas import tpu as pltpu
 from jax.sharding import PartitionSpec as P
+
+NY = 2
+UP, DOWN, ACROSS, SIBLING = range(4)
+
+
+class Gather:
+    def __init__(self, sizes, srcs, fulls, axes, send_sem, recv_sem, local_sem):
+        self.nf = sizes["fs"]
+        self.nz = self.nf // NY
+        self.rep, self.place, self.tp = lax.axis_index("rep"), lax.axis_index("fs"), lax.axis_index("tp")
+        self.z, self.y = self.place // NY, self.place % NY
+        self.srcs, self.fulls, self.axes = srcs, fulls, axes
+        self.send_sem, self.recv_sem, self.local_sem = send_sem, recv_sem, local_sem
+
+    def target(self, way):
+        rep, place = self.rep, self.place
+        if way == UP:
+            place = place + NY
+        elif way == DOWN:
+            place = place - NY
+        elif way == ACROSS:
+            place = self.z * NY + 1 - self.y
+        else:
+            rep = 1 - rep
+        return {"rep": rep, "fs": place, "tp": self.tp}
+
+    def view(self, ref, w, start, size):
+        axis = self.axes[w]
+        return ref.at[tuple([slice(None)] * axis + [pl.ds(start, size)])]
+
+    def piece(self, w, k, half):
+        rows = self.srcs[w].shape[self.axes[w]]
+        part = rows // 2
+        start = pl.multiple_of(k * rows + half * part, part)
+        return self.view(self.fulls[w], w, start, part)
+
+    def own_piece(self, w):
+        part = self.srcs[w].shape[self.axes[w]] // 2
+        return self.view(self.srcs[w], w, pl.multiple_of(self.rep * part, part), part)
+
+    def copy(self, w, k, way, own=False, half=None):
+        half = self.rep if half is None else half
+        return pltpu.make_async_remote_copy(
+            src_ref=self.own_piece(w) if own else self.piece(w, k, half),
+            dst_ref=self.piece(w, k, half),
+            send_sem=self.send_sem.at[way, w, k],
+            recv_sem=self.recv_sem.at[1 if way == SIBLING else 0, w, k],
+            device_id=self.target(way),
+            device_id_type=pl.DeviceIdType.MESH,
+        )
+
+    def barrier(self, others=()):
+        sem = pltpu.get_barrier_semaphore()
+
+        def greet(device):
+            pl.semaphore_signal(sem, inc=1, device_id=device, device_id_type=pl.DeviceIdType.MESH)
+
+        for way in (ACROSS, SIBLING):
+            greet(self.target(way))
+        for device in others:
+            greet(device)
+        pl.when(self.z > 0)(lambda: greet(self.target(DOWN)))
+        pl.when(self.z < self.nz - 1)(lambda: greet(self.target(UP)))
+        ends = (self.z > 0).astype(jnp.int32) + (self.z < self.nz - 1).astype(jnp.int32)
+        pl.semaphore_wait(sem, 2 + len(others) + ends)
+
+    def local(self, w):
+        rows = self.srcs[w].shape[self.axes[w]]
+        return pltpu.make_async_copy(
+            self.srcs[w], self.view(self.fulls[w], w, pl.multiple_of(self.place * rows, rows), rows), self.local_sem.at[w]
+        )
+
+    def own(self, w):
+        pl.when(self.z < self.nz - 1)(lambda: self.copy(w, self.place, UP, own=True).start())
+        pl.when(self.z > 0)(lambda: self.copy(w, self.place, DOWN, own=True).start())
+        self.copy(w, self.place, ACROSS, own=True).start()
+
+    def pass_on(self, w, k, ways):
+        self.copy(w, k, ACROSS).wait_recv()
+        for way in ways:
+            if way == UP:
+                pl.when(self.z < self.nz - 1)(lambda: self.copy(w, k, UP).start())
+            elif way == DOWN:
+                pl.when(self.z > 0)(lambda: self.copy(w, k, DOWN).start())
+            else:
+                self.copy(w, k, way).start()
+
+    def along(self, w, d):
+        pl.when(self.z >= d)(lambda: self.pass_on(w, (self.z - d) * NY + self.y, (UP, ACROSS, SIBLING)))
+        pl.when(self.z + d < self.nz)(lambda: self.pass_on(w, (self.z + d) * NY + self.y, (DOWN, ACROSS, SIBLING)))
+
+    def across(self, w, d):
+        other = 1 - self.y
+        pl.when(self.z >= d)(lambda: self.pass_on(w, (self.z - d) * NY + other, (SIBLING,)))
+        if d:
+            pl.when(self.z + d < self.nz)(lambda: self.pass_on(w, (self.z + d) * NY + other, (SIBLING,)))
+
+    def ready(self, w):
+        self.local(w).wait()
+
+        @pl.loop(0, self.nf)
+        def _(k):
+            pl.when(k != self.place)(lambda: self.copy(w, k, SIBLING, half=1 - self.rep).wait_recv())
+
+    def drain(self):
+        for w in range(len(self.srcs)):
+
+            @pl.loop(0, self.nf)
+            def _(k):
+                z, y = k // NY, k % NY
+                mine = y == self.y
+                pl.when(mine & (z <= self.z) & (self.z < self.nz - 1))(lambda: self.copy(w, k, UP).wait_send())
+                pl.when(mine & (z >= self.z) & (self.z > 0))(lambda: self.copy(w, k, DOWN).wait_send())
+                pl.when(mine)(lambda: self.copy(w, k, ACROSS).wait_send())
+                pl.when(k != self.place)(lambda: self.copy(w, k, SIBLING).wait_send())
+
+
+def gather_kernel(sizes, axes, *refs):
+    count = len(axes)
+    g = Gather(sizes, refs[:count], refs[count : 2 * count], axes, *refs[2 * count :])
+    for w in range(count):
+        g.local(w).start()
+    g.barrier()
+    g.own(0)
+    for w in range(count):
+        for d in range(1, g.nz):
+            g.along(w, d)
+            if d == 1 and w + 1 < count:
+                g.own(w + 1)
+            if w:
+                g.across(w - 1, d - 1)
+        if w:
+            g.across(w - 1, g.nz - 1)
+    for d in range(g.nz):
+        g.across(count - 1, d)
+    for w in range(count):
+        g.ready(w)
+    g.drain()
+
+
+def gather_all(sizes, weights, axes):
+    fulls = []
+    for weight, axis in zip(weights, axes):
+        shape = list(weight.shape)
+        shape[axis] *= sizes["fs"]
+        fulls.append(jax.ShapeDtypeStruct(tuple(shape), weight.dtype))
+    count = len(weights)
+    return pl.pallas_call(
+        functools.partial(gather_kernel, sizes, axes),
+        out_shape=fulls,
+        in_specs=[pl.BlockSpec(memory_space=pltpu.VMEM)] * count,
+        out_specs=[pl.BlockSpec(memory_space=pl.ANY)] * count,
+        scratch_shapes=[
+            pltpu.SemaphoreType.DMA((4, count, sizes["fs"])),
+            pltpu.SemaphoreType.DMA((2, count, sizes["fs"])),
+            pltpu.SemaphoreType.DMA((count,)),
+        ],
+        compiler_params=pltpu.CompilerParams(collective_id=0, has_side_effects=True),
+    )(*weights)
 
 
 def norm_rows(values, gain):
@@ -101,9 +264,94 @@
     return (middle + summed).astype(jnp.bfloat16).reshape(seq_count, kept_rows, model_width)
 
 
+def swap(values):
+    other = lax.ppermute(values, "tp", [(0, 1), (1, 0)])
+    first = lax.axis_index("tp") == 0
+    return jnp.stack([jnp.where(first, values, other), jnp.where(first, other, values)])
+
+
+def paired_device(
+    sizes,
+    tokens,
+    mixer_gain,
+    value_weight,
+    value_scale,
+    gate_weight,
+    gate_scale,
+    pool_weight,
+    pool_scale,
+    channel_gain,
+    up_weight,
+    up_scale,
+    down_weight,
+    down_scale,
+):
+    seq_count, seq_length, model_width = tokens.shape
+    shares = lax.axis_size("tp")
+    member = lax.axis_index("tp")
+    kept_rows = seq_length // shares
+    group_count, local_width = value_scale.shape
+    rows = value_weight.shape[0]
+    value_full, gate_full, pool_full, up_full, down_full = gather_all(
+        sizes,
+        (
+            value_weight.astype(jnp.bfloat16).reshape(rows, -1),
+            gate_weight.astype(jnp.bfloat16).reshape(rows, -1),
+            pool_weight.astype(jnp.bfloat16),
+            up_weight.astype(jnp.bfloat16),
+            down_weight.astype(jnp.bfloat16).T,
+        ),
+        (0, 0, 1, 0, 0),
+    )
+    down_scales = lax.all_gather(down_scale, "fs", axis=0, tiled=True)
+    outs = []
+    for tokens_here in tokens:
+        normed = norm_rows(tokens_here, mixer_gain).astype(jnp.bfloat16)
+        value = jnp.dot(normed, value_full, preferred_element_type=jnp.float32)
+        value = (value * value_scale.reshape(-1)).astype(jnp.bfloat16)
+        gating = jnp.dot(normed, gate_full, preferred_element_type=jnp.float32) * gate_scale.reshape(-1)
+        excess = pool_excess(value.reshape(1, seq_length, group_count, local_width)).astype(jnp.bfloat16)
+        both = swap(excess[0].reshape(seq_length, -1))
+        merged = []
+        for group in range(group_count):
+            cut = slice(group * local_width, (group + 1) * local_width)
+            pooled = jnp.dot(
+                jnp.concatenate([both[i][:, cut] for i in range(shares)], axis=1),
+                pool_full[group],
+                preferred_element_type=jnp.float32,
+            )
+            merged.append((jax.nn.sigmoid(gating[:, cut]) * (pooled * pool_scale[group])).astype(jnp.bfloat16))
+        merged = swap(jnp.concatenate(merged, axis=1))
+        merged = jnp.concatenate(
+            [
+                merged[i][:, group * local_width : (group + 1) * local_width]
+                for group in range(group_count)
+                for i in range(shares)
+            ],
+            axis=1,
+        )
+        middle = tokens_here.astype(jnp.float32) + merged.astype(jnp.float32)
+        normed_two = norm_rows(middle, channel_gain).astype(jnp.bfloat16)
+        upward = jnp.dot(normed_two, up_full, preferred_element_type=jnp.float32) * up_scale
+        hidden = jnp.square(jax.nn.relu(upward)).astype(jnp.bfloat16)
+        part = (
+            lax.dot_general(hidden, down_full, (((1,), (1,)), ((), ())), preferred_element_type=jnp.float32)
+            * down_scales
+        ).astype(jnp.bfloat16)
+        theirs = lax.dynamic_slice_in_dim(part, (1 - member) * kept_rows, kept_rows, 0)
+        mine = lax.dynamic_slice_in_dim(part, member * kept_rows, kept_rows, 0)
+        got = lax.ppermute(theirs, "tp", [(0, 1), (1, 0)])
+        summed = mine.astype(jnp.float32) + got.astype(jnp.float32)
+        own = lax.dynamic_slice_in_dim(middle, member * kept_rows, kept_rows, 0)
+        outs.append((own + summed).astype(jnp.bfloat16))
+    return jnp.stack(outs)
+
+
 def solution(mesh):
+    sizes = dict(mesh.shape)
+    paired = sizes["rep"] == 2 and sizes["tp"] == 2 and sizes["fs"] % NY == 0 and sizes["fs"] <= 16
     return jax.shard_map(
-        per_device,
+        functools.partial(paired_device, sizes) if paired else per_device,
         mesh=mesh,
         in_specs=(
             P(("rep", "fs"), None, None),

time: 647 us -> 341 us (0.53)
  waiting for transfers between devices: 519 us -> 82.4 us
  Pallas kernels: 0 us -> 154 us
  local copies, waits for them, and re-layouts: 28.8 us -> 14.6 us
  between operations: 13.7 us -> 0.37 us
  other arithmetic: 21.9 us -> 31 us
    all_gather x7 -> x0, waiting for transfers between devices: 459 us -> none  [the longest x1 126 us: per_device(): lax.all_gather(up_weight.astype(jnp.bfloat16), 'fs', axis=0, tiled=True)]
    pallas_call x0 -> x1, Pallas kernels: none -> 154 us  [gather_all(): pl.pallas_call(functools.partial(gather_kernel, sizes, axes), out_shape=f...]
    ppermute x0 -> x3, waiting for transfers between devices: none -> 82.4 us  [the longest x2 48 us: swap(): other = lax.ppermute(values, 'tp', [(0, 1), (1, 0)])]
    reduce_scatter x1 -> x0, waiting for transfers between devices: 41.8 us -> none  [per_device(): lax.psum_scatter((jnp.dot(rows_part, down_full, preferred_element_type=jn...]
    all_to_all x1 -> x0, waiting for transfers between devices: 19 us -> none  [per_device(): lax.all_to_all(merged, 'tp', split_axis=1, concat_axis=3, tiled=True)]
    another operation x1 -> x2, other arithmetic: 0.76 us -> 11.8 us
    convert_element_type x3 -> x0, local copies, waits for them, and re-layouts: 10.6 us -> none  [the longest x2 8.2 us: per_device(): merged_own.reshape(seq_count * kept_rows, model_width).astype(jnp.float32)]
    convert_element_type x6 -> x4, other arithmetic: 12.2 us -> 3.52 us  [the longest x1 1.56 us: paired_device(): value_weight.astype(jnp.bfloat16).reshape(rows, -1)]
  transfers between devices with their start and end apart: 9 -> 3, of which waited for: 9 -> 3; matrix products, arithmetic and copies ran while one was open for 8% -> 2% of each run, Pallas kernels for 0% -> 0%
where the time goes in v1:
time: 341 us
  Pallas kernels  154 us (45%)
  waiting for transfers between devices  82.4 us (24%)
  matrix products  35.7 us (10%)
  other arithmetic  31 us (9%)
  blocking collectives  17.7 us (5%)
  local copies, waits for them, and re-layouts  14.6 us (4%)
  starting transfers between devices  4.51 us (1%)
    pallas_call x1, Pallas kernels, gather_all(): pl.pallas_call(functools.partial(gather_kernel, sizes, axes), out_shape=f...  154 us
    ppermute x2, waiting for transfers between devices, swap(): other = lax.ppermute(values, 'tp', [(0, 1), (1, 0)])  48 us
    ppermute x1, waiting for transfers between devices, paired_device(): got = lax.ppermute(theirs, 'tp', [(0, 1), (1, 0)])  34.4 us
    dot_general x1, matrix products, paired_device(): lax.dot_general(hidden, down_full, (((1,), (1,)), ((), ())), preferred_el...  21.5 us
    all_gather x1, blocking collectives, paired_device(): down_scales = lax.all_gather(down_scale, 'fs', axis=0, tiled=True)  17.7 us
    another operation x1, other arithmetic  7.55 us
    unnamed x49, local copies, waits for them, and re-layouts  7.54 us
    dot_general x1, matrix products, paired_device(): value = jnp.dot(normed, value_full, preferred_element_type=jnp.float32)  7.33 us
  transfers between devices with their start and end apart: 3, of which 3 were waited for; matrix products, arithmetic and copies ran while one was open for 2% of the time, Pallas kernels for 0%

profile of v1, /device:TPU:0, one launch (start us, length us, event | category | flops | bytes accessed | tf_op | source)
XLA Modules:
  0.0 340.6 jit_solution(6926739237581013955)
XLA Ops:
  0.0 1.6 convert_element_type.121
  1.6 0.9 copy.28
  2.7 0.9 copy.29
  3.6 0.7 convert_element_type.123.refs_2_
  4.3 1.1 convert_element_type.124.refs_3_
  5.4 2.8 copy.19
  8.1 0.7 fusion
  8.9 154.4 %shard_map.127 = (bf16[2048,1024]{1,0:T(8,128)(2,1)}, bf16[2048,1024]{1,0:T(8,128)(2,1)}, bf16[4,512,256]{2,1,0:T(8,128)(2,1)}, bf16[2048,2048]{1,0:T(8,128)(2,1)}, bf16[2048,2048]{1,0:T(8,128)(2,1)}) custom-call(bf16[256,1024]{1,0:T(8,128)(2,1)} %bitcast.53, bf16[256,1024]{1,0:T(8,128)(2,1)} %bitcast.54, bf16[4,64,256]{2,1,0:T(8,128)(2,1)} %convert_element_type.123.refs_2_, ...), custom_call_target="tpu_custom_call" | custom-call | tf_op jit(solution)/shard_map/pallas_call | solution.py:156
  163.3 7.3 %fusion.12 = f32[768,1024]{1,0:T(8,128)} fusion(bf16[2048,1024]{1,0:T(8,128)(2,1)} %get-tuple-element.11, f32[1024]{0:T(1024)S(1)} %bitcast.61, bf16[1,768,2048]{2,1,0:T(8,128)(2,1)S(1)} %copy-done, f32[2048]{0:T(1024)S(1)} %copy-done.15, f32[768]{0:T(1024)S(1)} %add_rsqrt_fusion.1), kind=kOutput, calls=%fused_computation.24 | convolution fusion | flops 3229876224 | bytes 10501120 | tf_op jit(solution)/shard_map/dot_general | solution.py:310
  170.6 3.4 %reshape.129 = f32[1,768,4,256]{3,2,1,0:T(4,128)S(1)} reshape(f32[768,1024]{1,0:T(8,128)} %fusion.12) | data formatting | bytes 6291456 | tf_op jit(solution)/shard_map/convert_element_type | solution.py:176
  174.0 0.5 fusion.3
  174.6 0.5 fusion.4
  175.1 0.5 fusion.5
  176.2 7.5 %fusion.50 = (bf16[1,768,1,256]{3,2,1,0:T(2,128)(2,1)S(1)}, bf16[1,768,1,256]{3,2,1,0:T(2,128)(2,1)S(1)}, bf16[1,768,1,256]{3,2,1,0:T(2,128)(2,1)S(1)}, bf16[1,768,1,256]{3,2,1,0:T(2,128)(2,1)S(1)}) fusion(f32[1,768,4,256]{3,2,1,0:T(4,128)S(1)} %reshape.129, f32[1,768,4,256]{3,2,1,0:T(4,128)S(1)} %fusion.5, f32[768]{0:T(1024)S(1)} %get-tuple-element.38, ...), kind=kLoop, calls=%fused_computation.80 | loop fusion | flops 2555904 | bytes 8663040 | tf_op jit(solution)/shard_map/convert.4
  183.8 3.7 %pad_maximum_fusion = bf16[1,768,4,256]{3,2,1,0:T(4,128)(2,1)S(1)} fusion(bf16[1,768,1,256]{3,2,1,0:T(2,128)(2,1)S(1)} %get-tuple-element.18, bf16[1,768,1,256]{3,2,1,0:T(2,128)(2,1)S(1)} %get-tuple-element.17, bf16[1,768,1,256]{3,2,1,0:T(2,128)(2,1)S(1)} %get-tuple-element.24, bf16[1,768,1,256]{3,2,1,0:T(2,128)(2,1)S(1)} %get-tuple-element.23), kind=kLoop, calls=%fused_computation.26 | loop fusion | flops 6291456 | bytes 3145728 | tf_op jit(solution)/shard_map/stack | solution.py:186
  187.5 1.5 copy.32
  189.0 1.5 collective-permute-start
  190.6 5.3 %convolution_multiply_fusion = f32[768,1024]{1,0:T(8,128)S(1)} fusion(bf16[2048,1024]{1,0:T(8,128)(2,1)} %get-tuple-element.10, f32[1024]{0:T(1024)S(1)} %bitcast.60, bf16[1,768,2048]{2,1,0:T(8,128)(2,1)S(1)} %copy-done.1, f32[2048]{0:T(1024)S(1)} %copy-done.15, f32[768]{0:T(1024)S(1)} %add_rsqrt_fusion.1), kind=kOutput, calls=%fused_computation.23 | convolution fusion | flops 3228303360 | bytes 10501120 | tf_op jit(solution)/shard_map/dot_general | solution.py:312
  195.9 30.5 %collective-permute-done = bf16[768,1024]{1,0:T(8,128)(2,1)} collective-permute-done((bf16[768,1024]{1,0:T(8,128)(2,1)}, bf16[768,1024]{1,0:T(8,128)(2,1)}, u32[]{:S(2)}, u32[]{:S(2)}) %collective-permute-start) | collective-permute-done | bytes 1572896 | tf_op jit(solution)/shard_map/ppermute | solution.py:268
  226.4 2.1 broadcast_select_fusion.3
  228.7 1.0 copy-done.14
  231.3 1.4 pad_maximum_fusion.1
  232.6 1.5 collective-permute-start.1
  234.1 17.7 %all-gather = f32[8,1,256]{2,1,0:T(1,128)S(1)} all-gather(f32[1,1,256]{2,1,0:T(1,128)S(1)} %bitcast.62), channel_id=1, replica_groups=mesh['rep'=2,'fs'=8,'tp'=2] {'fs'}, dimensions={0}, use_global_device_ids=true | all-gather | bytes 9216 | tf_op jit(solution)/shard_map/all_gather | solution.py:306
  251.9 17.5 %collective-permute-done.1 = bf16[768,1024]{1,0:T(8,128)(2,1)} collective-permute-done((bf16[768,1024]{1,0:T(8,128)(2,1)}, bf16[768,1024]{1,0:T(8,128)(2,1)}, u32[]{:S(2)}, u32[]{:S(2)}) %collective-permute-start.1) | collective-permute-done | bytes 1572896 | tf_op jit(solution)/shard_map/ppermute | solution.py:268
  269.4 2.4 broadcast_select_fusion
  272.3 3.7 %convert_add_fusion = (f32[768,2048]{1,0:T(8,128)}, f32[768]{0:T(1024)S(1)}) fusion(bf16[768,2048]{1,0:T(8,128)(2,1)S(1)} %slice_dynamic-update-slice_fusion, bf16[1,768,2048]{2,1,0:T(8,128)(2,1)S(1)} %copy-done.1), kind=kLoop, calls=%fused_computation | loop fusion | flops 7863552 | bytes 12585984 | tf_op jit(solution)/shard_map/add | solution.py:333
  276.1 21.5 %multiply_convert_fusion = bf16[768,2048]{1,0:T(8,128)(2,1)} fusion(bf16[2048,2048]{1,0:T(8,128)(2,1)} %get-tuple-element.14, bf16[2048,2048]{1,0:T(8,128)(2,1)} %get-tuple-element.13, f32[2048]{0:T(1024)S(1)} %bitcast.57, f32[2048]{0:T(1024)S(1)} %copy-done.16, f32[2048]{0:T(1024)S(1)} %copy-done.17, f32[768]{0:T(1024)S(1)} %add_rsqrt_fusion, ...), kind=kOutput, calls=%fused_computation.6 | convolution fusion | flops 12903776256 | bytes 26242048 | tf_op jit(solution)/shard_map/dot_general | solution.py:338
  297.6 2.9 constant_dynamic-slice_fusion
  300.5 1.5 collective-permute-start.2
  302.0 34.4 %collective-permute-done.2 = bf16[384,2048]{1,0:T(8,128)(2,1)} collective-permute-done((bf16[384,2048]{1,0:T(8,128)(2,1)}, bf16[384,2048]{1,0:T(8,128)(2,1)}, u32[]{:S(2)}, u32[]{:S(2)}) %collective-permute-start.2) | collective-permute-done | bytes 1572896 | tf_op jit(solution)/shard_map/ppermute | solution.py:343
  336.4 4.3 %fusion.13 = bf16[1,384,2048]{2,1,0:T(8,128)(2,1)} fusion(bf16[384,2048]{1,0:T(8,128)(2,1)} %collective-permute-done.2, f32[768,2048]{1,0:T(8,128)} %get-tuple-element.15, s32[]{:T(128)S(6)} %select_n.32, bf16[768,2048]{1,0:T(8,128)(2,1)S(1)} %copy-done.3), kind=kLoop, calls=%fused_computation.25 | loop fusion | flops 3932160 | bytes 7864324 | tf_op jit(solution)/shard_map/stack | solution.py:347
  (58 shorter events, 3.0 us)
Async XLA Ops:
  0.0 2.5 copy-start.8
  0.0 3.6 %copy-start.9 = (f32[4,64,256]{2,1,0:T(8,128)S(1)}, f32[4,64,256]{2,1,0:T(8,128)}, u32[]{:S(2)}) copy-start(f32[4,64,256]{2,1,0:T(8,128)} %param.19) | copy-start | bytes 786436
  0.0 4.2 %copy-start.4 = (f32[256,2048]{1,0:T(8,128)S(1)}, f32[256,2048]{1,0:T(8,128)}, u32[]{:S(2)}) copy-start(f32[256,2048]{1,0:T(8,128)} %param.22) | copy-start | bytes 6291460
  4.3 3.9 %copy-start = (bf16[1,768,2048]{2,1,0:T(8,128)(2,1)S(1)}, bf16[1,768,2048]{2,1,0:T(8,128)(2,1)}, u32[]{:S(2)}) copy-start(bf16[1,768,2048]{2,1,0:T(8,128)(2,1)} %param.13) | copy-start | bytes 9437188
  5.4 3.5 %copy-start.10 = (f32[4,256]{1,0:T(4,128)S(1)}, f32[4,256]{1,0:T(4,128)}, u32[]{:S(2)}) copy-start(f32[4,256]{1,0:T(4,128)} %param.16) | copy-start | bytes 12292
  8.1 155.1 %copy-start.15 = (f32[2048]{0:T(1024)S(1)}, f32[2048]{0:T(1024)}, u32[]{:S(2)}) copy-start(f32[2048]{0:T(1024)} %param.14) | copy-start | bytes 24580
  183.8 6.7 %copy-start.11 = (f32[4,256]{1,0:T(4,128)S(1)}, f32[4,256]{1,0:T(4,128)}, u32[]{:S(2)}) copy-start(f32[4,256]{1,0:T(4,128)} %param.18) | copy-start | bytes 12292
  183.8 6.7 %copy-start.12 = (f32[4,256]{1,0:T(4,128)S(1)}, f32[4,256]{1,0:T(4,128)}, u32[]{:S(2)}) copy-start(f32[4,256]{1,0:T(4,128)} %param.20) | copy-start | bytes 12292
  183.8 6.7 %copy-start.1 = (bf16[1,768,2048]{2,1,0:T(8,128)(2,1)S(1)}, bf16[1,768,2048]{2,1,0:T(8,128)(2,1)}, u32[]{:S(2)}) copy-start(bf16[1,768,2048]{2,1,0:T(8,128)(2,1)} %param.13) | copy-start | bytes 9437188
  189.0 37.4 %collective-permute-start = (bf16[768,1024]{1,0:T(8,128)(2,1)}, bf16[768,1024]{1,0:T(8,128)(2,1)}, u32[]{:S(2)}, u32[]{:S(2)}) collective-permute-start(bf16[768,1024]{1,0:T(8,128)(2,1)} %bitcast.24), channel_id=1, source_target_pairs={{0,1},{1,0},{2,3},{3,2},{4,5},{5,4},{6,7},{7,6},{8,9},{9,8},{10,11... | collective-permute-start | bytes 4718600 | tf_op jit(solution)/shard_map/ppermute | solution.py:268
  228.5 1.2 copy-start.14
  230.5 0.8 copy-start.5
  230.8 1.8 copy-start.6
  230.9 3.3 copy-start.13
  231.2 1.4 copy-start.7
  232.6 36.7 %collective-permute-start.1 = (bf16[768,1024]{1,0:T(8,128)(2,1)}, bf16[768,1024]{1,0:T(8,128)(2,1)}, u32[]{:S(2)}, u32[]{:S(2)}) collective-permute-start(bf16[768,1024]{1,0:T(8,128)(2,1)} %pad_maximum_fusion.1), channel_id=1, source_target_pairs={{0,1},{1,0},{2,3},{3,2},{4,5},{5,4},{6,7},{7,6},{8,9},{9,8},{10,11... | collective-permute-start | bytes 4718600 | tf_op jit(solution)/shard_map/ppermute | solution.py:268
  272.3 3.7 %copy-start.2 = (bf16[768,2048]{1,0:T(8,128)(2,1)}, bf16[768,2048]{1,0:T(8,128)(2,1)S(1)}, u32[]{:S(2)}) copy-start(bf16[768,2048]{1,0:T(8,128)(2,1)S(1)} %slice_dynamic-update-slice_fusion) | copy-start | bytes 9437188
  272.3 3.7 %copy-start.16 = (f32[2048]{0:T(1024)S(1)}, f32[2048]{0:T(1024)}, u32[]{:S(2)}) copy-start(f32[2048]{0:T(1024)} %param.23) | copy-start | bytes 24580
  272.3 3.7 %copy-start.17 = (f32[2048]{0:T(1024)S(1)}, f32[2048]{0:T(1024)}, u32[]{:S(2)}) copy-start(f32[2048]{0:T(1024)} %param.21) | copy-start | bytes 24580
  297.6 38.8 %copy-start.3 = (bf16[768,2048]{1,0:T(8,128)(2,1)S(1)}, bf16[768,2048]{1,0:T(8,128)(2,1)}, u32[]{:S(2)}) copy-start(bf16[768,2048]{1,0:T(8,128)(2,1)} %multiply_convert_fusion) | copy-start | bytes 9437188
  300.5 35.9 %collective-permute-start.2 = (bf16[384,2048]{1,0:T(8,128)(2,1)}, bf16[384,2048]{1,0:T(8,128)(2,1)}, u32[]{:S(2)}, u32[]{:S(2)}) collective-permute-start(bf16[384,2048]{1,0:T(8,128)(2,1)} %constant_dynamic-slice_fusion), channel_id=1, source_target_pairs={{0,1},{1,0},{2,3},{3,2},{4,5},{5,4},{6,7},{7,6},{8,9},{9,8},{10,11... | collective-permute-start | bytes 4718600 | tf_op jit(solution)/shard_map/ppermute | solution.py:343

commit v2 on v1

--- a/solution.py
+++ b/solution.py
@@ -42,14 +42,10 @@
         start = pl.multiple_of(k * rows + half * part, part)
         return self.view(self.fulls[w], w, start, part)
 
-    def own_piece(self, w):
-        part = self.srcs[w].shape[self.axes[w]] // 2
-        return self.view(self.srcs[w], w, pl.multiple_of(self.rep * part, part), part)
-
-    def copy(self, w, k, way, own=False, half=None):
+    def copy(self, w, k, way, half=None):
         half = self.rep if half is None else half
         return pltpu.make_async_remote_copy(
-            src_ref=self.own_piece(w) if own else self.piece(w, k, half),
+            src_ref=self.piece(w, k, half),
             dst_ref=self.piece(w, k, half),
             send_sem=self.send_sem.at[way, w, k],
             recv_sem=self.recv_sem.at[1 if way == SIBLING else 0, w, k],
@@ -79,9 +75,9 @@
         )
 
     def own(self, w):
-        pl.when(self.z < self.nz - 1)(lambda: self.copy(w, self.place, UP, own=True).start())
-        pl.when(self.z > 0)(lambda: self.copy(w, self.place, DOWN, own=True).start())
-        self.copy(w, self.place, ACROSS, own=True).start()
+        pl.when(self.z < self.nz - 1)(lambda: self.copy(w, self.place, UP).start())
+        pl.when(self.z > 0)(lambda: self.copy(w, self.place, DOWN).start())
+        self.copy(w, self.place, ACROSS).start()
 
     def pass_on(self, w, k, ways):
         self.copy(w, k, ACROSS).wait_recv()
@@ -104,8 +100,6 @@
             pl.when(self.z + d < self.nz)(lambda: self.pass_on(w, (self.z + d) * NY + other, (SIBLING,)))
 
     def ready(self, w):
-        self.local(w).wait()
-
         @pl.loop(0, self.nf)
         def _(k):
             pl.when(k != self.place)(lambda: self.copy(w, k, SIBLING, half=1 - self.rep).wait_recv())
@@ -123,48 +117,247 @@
                 pl.when(k != self.place)(lambda: self.copy(w, k, SIBLING).wait_send())
 
 
-def gather_kernel(sizes, axes, *refs):
-    count = len(axes)
-    g = Gather(sizes, refs[:count], refs[count : 2 * count], axes, *refs[2 * count :])
+VALUE, GATE, POOL, SCALES, HIDE, SHOW = range(6)
+AXES = (0, 0, 1, 0, 0, 0)
+
+
+def layer_kernel(sizes, *refs):
+    count = len(AXES)
+    tokens, mixer_gain, value_scale, gate_scale, pool_scale, channel_gain, up_scale = refs[:7]
+    srcs, out, fulls = refs[7 : 7 + count], refs[7 + count], refs[8 + count : 8 + 2 * count]
+    normed, excess, excess_in, gate, merged, merged_in, hidden, part_out, part_own, part_in = refs[
+        8 + 2 * count : 18 + 2 * count
+    ]
+    send_sem, recv_sem, local_sem, pair_send, pair_recv = refs[18 + 2 * count :]
+    g = Gather(sizes, srcs, fulls, AXES, send_sem, recv_sem, local_sem)
+    rows, width = tokens.shape
+    groups, _, local = excess.shape
+    half = rows // 2
+    member = g.tp
+    partner = {"rep": g.rep, "fs": g.place, "tp": 1 - member}
+
+    def pair_copy(kind, index, source, target):
+        return pltpu.make_async_remote_copy(
+            src_ref=source.at[index],
+            dst_ref=target.at[index],
+            send_sem=pair_send.at[kind, index],
+            recv_sem=pair_recv.at[kind, index],
+            device_id=partner,
+            device_id_type=pl.DeviceIdType.MESH,
+        )
+
+    def excess_copy(group):
+        return pair_copy(0, group, excess, excess_in)
+
+    def merged_copy(group):
+        return pair_copy(1, group, merged, merged_in)
+
+    def part_copy(k):
+        return pair_copy(2, k, part_out, part_in)
+
+    def norm_in():
+        @pl.loop(0, rows // 16)
+        def _(i):
+            at = pl.ds(pl.multiple_of(i * 16, 16), 16)
+            normed[at, :] = norm_rows(tokens[at, :], mixer_gain[...]).astype(jnp.bfloat16)
+
+    def value_piece(group):
+        cut = pl.ds(group * local, local)
+        value = jnp.dot(normed[...], fulls[VALUE][:, cut], preferred_element_type=jnp.float32) * value_scale[:, cut]
+        floats = value.astype(jnp.bfloat16).astype(jnp.float32)
+        place = lax.broadcasted_iota(jnp.int32, floats.shape, 0)
+        running = floats
+        for level in range(group + 1):
+            shifted = pltpu.roll(running, 2**level, 0)
+            running = running + jnp.where(place >= 2**level, shifted, 0.0)
+        counts = jnp.minimum(place + 1, 2 ** (group + 1)).astype(jnp.float32)
+        excess[group] = (running / counts - floats).astype(jnp.bfloat16)
+        excess_copy(group).start()
+
+    def gate_piece(group):
+        cut = pl.ds(group * local, local)
+
+        @pl.loop(0, 2)
+        def _(i):
+            at = pl.ds(pl.multiple_of(i * half, half), half)
+            value = jnp.dot(normed[at, :], fulls[GATE][:, cut], preferred_element_type=jnp.float32)
+            gate[group, at, :] = jax.nn.sigmoid(value * gate_scale[:, cut])
+
+    def pool_piece(group):
+        excess_copy(group).wait_recv()
+        weight = fulls[POOL].at[group]
+        mine = weight[pl.ds(pl.multiple_of(member * local, local), local), :]
+        theirs = weight[pl.ds(pl.multiple_of((1 - member) * local, local), local), :]
+        pooled = jnp.dot(excess[group], mine, preferred_element_type=jnp.float32) + jnp.dot(
+            excess_in[group], theirs, preferred_element_type=jnp.float32
+        )
+        scale = pool_scale[:, pl.ds(group * local, local)]
+        merged[group] = (gate[group] * (pooled * scale)).astype(jnp.bfloat16)
+        merged_copy(group).start()
+
+    def slabs(at):
+        for group in range(groups):
+            for source, owner in ((merged, member), (merged_in, 1 - member)):
+                cut = pl.ds(pl.multiple_of((2 * group + owner) * local, local), local)
+                yield cut, tokens[at, cut].astype(jnp.float32) + source[group, at, :].astype(jnp.float32)
+
+    def norm_mid(part, parts):
+        if part == 0:
+            for group in range(groups):
+                merged_copy(group).wait_recv()
+        steps = rows // 16 // parts
+
+        @pl.loop(part * steps, (part + 1) * steps)
+        def _(i):
+            at = pl.ds(pl.multiple_of(i * 16, 16), 16)
+            held = list(slabs(at))
+            total = sum(jnp.sum(values * values, axis=-1, keepdims=True) for _, values in held)
+            factor = lax.rsqrt(total / width + 1e-06)
+            for cut, values in held:
+                normed[at, cut] = (values * factor * channel_gain[:, cut]).astype(jnp.bfloat16)
+
+    def up_piece(n):
+        cut = pl.ds(n * local, local)
+
+        @pl.loop(0, 2)
+        def _(i):
+            at = pl.ds(pl.multiple_of(i * half, half), half)
+            upward = jnp.dot(normed[at, :], fulls[HIDE][:, cut], preferred_element_type=jnp.float32) * up_scale[:, cut]
+            hidden[at, cut] = jnp.square(jax.nn.relu(upward)).astype(jnp.bfloat16)
+
+    inner = hidden.shape[1]
+
+    def down_piece(k, first):
+        weight = fulls[SHOW][pl.ds(pl.multiple_of(k * inner, inner), inner), :]
+        scale = fulls[SCALES][pl.ds(pl.multiple_of(k * 16, 16), 16), :][:1]
+        at = pl.ds(pl.multiple_of(first, half), half)
+        part = jnp.dot(hidden[at, :], weight, preferred_element_type=jnp.float32) * scale
+        return part.astype(jnp.bfloat16)
+
+    def finish():
+        wide = fulls[SHOW].shape[1]
+
+        @pl.loop(0, g.nf)
+        def _(k):
+            part_out[k] = down_piece(k, (1 - member) * half)
+            part_copy(k).start()
+
+        @pl.loop(0, g.nf)
+        def _(k):
+            part_own[k] = down_piece(k, member * half)
+
+        @pl.loop(0, g.nf)
+        def _(k):
+            part_copy(k).wait_recv()
+
+        @pl.loop(0, g.nf)
+        def _(k):
+            cut = pl.ds(pl.multiple_of(k * wide, wide), wide)
+            summed = part_own[k].astype(jnp.float32) + part_in[k].astype(jnp.float32)
+            out[:, cut] = (middle_of(k) + summed).astype(out.dtype)
+
+    def middle_of(k):
+        group, owner = k // 2, k % 2
+        cut = pl.ds(pl.multiple_of(k * local, local), local)
+        at = pl.ds(pl.multiple_of(member * half, half), half)
+        own = merged[group, at, :].astype(jnp.float32)
+        other = merged_in[group, at, :].astype(jnp.float32)
+        return tokens[at, cut].astype(jnp.float32) + jnp.where(owner == member, own, other)
+
+    work = []
+
+    def emit(n):
+        for _ in range(min(n, len(work))):
+            work.pop(0)()
+
+    def queue(w):
+        g.ready(w)
+        if w == VALUE:
+            work.extend(functools.partial(value_piece, i) for i in range(groups))
+        elif w == GATE:
+            work.extend(functools.partial(gate_piece, i) for i in range(groups))
+        elif w == SCALES:
+            work.extend(functools.partial(pool_piece, i) for i in range(groups))
+            work.extend(functools.partial(norm_mid, i, 3) for i in range(3))
+        elif w == HIDE:
+            work.extend(functools.partial(up_piece, i) for i in range(inner // local))
+
     for w in range(count):
         g.local(w).start()
-    g.barrier()
+    g.barrier((partner,))
+    for w in range(count):
+        g.local(w).wait()
     g.own(0)
+    norm_in()
     for w in range(count):
         for d in range(1, g.nz):
             g.along(w, d)
-            if d == 1 and w + 1 < count:
-                g.own(w + 1)
-            if w:
-                g.across(w - 1, d - 1)
-        if w:
-            g.across(w - 1, g.nz - 1)
-    for d in range(g.nz):
-        g.across(count - 1, d)
-    for w in range(count):
-        g.ready(w)
+            if d == 1:
+                if w + 1 < count:
+                    g.own(w + 1)
+                if w:
+                    g.across(w - 1, g.nz - 1)
+                    queue(w - 1)
+            else:
+                g.across(w, d - 2)
+            emit(2)
+        g.across(w, g.nz - 2)
+        emit(2)
+    g.across(count - 1, g.nz - 1)
+    emit(len(work))
+    g.ready(count - 1)
+    finish()
+    for group in range(groups):
+        excess_copy(group).wait_send()
+        merged_copy(group).wait_send()
+
+    @pl.loop(0, g.nf)
+    def _(k):
+        part_copy(k).wait_send()
+
     g.drain()
 
 
-def gather_all(sizes, weights, axes):
+def run_layer(sizes, tokens, vectors, weights):
+    rows, width = tokens.shape
+    count = len(weights)
     fulls = []
-    for weight, axis in zip(weights, axes):
+    for weight, axis in zip(weights, AXES):
         shape = list(weight.shape)
         shape[axis] *= sizes["fs"]
-        fulls.append(jax.ShapeDtypeStruct(tuple(shape), weight.dtype))
-    count = len(weights)
+        fulls.append(pltpu.VMEM(tuple(shape), weight.dtype))
+    groups, _, local = weights[POOL].shape
+    inner, wide = weights[SHOW].shape
+    halves = (sizes["fs"], rows // 2, wide)
+    pieces = (groups, rows, local)
     return pl.pallas_call(
-        functools.partial(gather_kernel, sizes, axes),
-        out_shape=fulls,
-        in_specs=[pl.BlockSpec(memory_space=pltpu.VMEM)] * count,
-        out_specs=[pl.BlockSpec(memory_space=pl.ANY)] * count,
-        scratch_shapes=[
+        functools.partial(layer_kernel, sizes),
+        out_shape=jax.ShapeDtypeStruct((rows // 2, width), jnp.bfloat16),
+        in_specs=[pl.BlockSpec(memory_space=pltpu.VMEM)] * (1 + len(vectors))
+        + [pl.BlockSpec(memory_space=pl.ANY)] * count,
+        out_specs=pl.BlockSpec(memory_space=pltpu.VMEM),
+        scratch_shapes=fulls
+        + [
+            pltpu.VMEM((rows, width), jnp.bfloat16),
+            pltpu.VMEM(pieces, jnp.bfloat16),
+            pltpu.VMEM(pieces, jnp.bfloat16),
+            pltpu.VMEM(pieces, jnp.float32),
+            pltpu.VMEM(pieces, jnp.bfloat16),
+            pltpu.VMEM(pieces, jnp.bfloat16),
+            pltpu.VMEM((rows, inner), jnp.bfloat16),
+            pltpu.VMEM(halves, jnp.bfloat16),
+            pltpu.VMEM(halves, jnp.bfloat16),
+            pltpu.VMEM(halves, jnp.bfloat16),
             pltpu.SemaphoreType.DMA((4, count, sizes["fs"])),
             pltpu.SemaphoreType.DMA((2, count, sizes["fs"])),
             pltpu.SemaphoreType.DMA((count,)),
+            pltpu.SemaphoreType.DMA((3, 8)),
+            pltpu.SemaphoreType.DMA((3, 8)),
         ],
-        compiler_params=pltpu.CompilerParams(collective_id=0, has_side_effects=True),
-    )(*weights)
+        compiler_params=pltpu.CompilerParams(
+            collective_id=0, has_side_effects=True, vmem_limit_bytes=63 * 2**20
+        ),
+    )(tokens, *vectors, *weights)
 
 
 def norm_rows(values, gain):
@@ -264,12 +457,6 @@
     return (middle + summed).astype(jnp.bfloat16).reshape(seq_count, kept_rows, model_width)
 
 
-def swap(values):
-    other = lax.ppermute(values, "tp", [(0, 1), (1, 0)])
-    first = lax.axis_index("tp") == 0
-    return jnp.stack([jnp.where(first, values, other), jnp.where(first, other, values)])
-
-
 def paired_device(
     sizes,
     tokens,
@@ -286,72 +473,43 @@
     down_weight,
     down_scale,
 ):
-    seq_count, seq_length, model_width = tokens.shape
-    shares = lax.axis_size("tp")
-    member = lax.axis_index("tp")
-    kept_rows = seq_length // shares
-    group_count, local_width = value_scale.shape
     rows = value_weight.shape[0]
-    value_full, gate_full, pool_full, up_full, down_full = gather_all(
+    row = lambda vector: vector.reshape(1, -1)
+    out = run_layer(
         sizes,
+        tokens[0],
+        (
+            row(mixer_gain),
+            row(value_scale),
+            row(gate_scale),
+            row(pool_scale),
+            row(channel_gain),
+            row(up_scale),
+        ),
         (
             value_weight.astype(jnp.bfloat16).reshape(rows, -1),
             gate_weight.astype(jnp.bfloat16).reshape(rows, -1),
             pool_weight.astype(jnp.bfloat16),
+            jnp.broadcast_to(row(down_scale), (16, down_scale.shape[0])),
             up_weight.astype(jnp.bfloat16),
-            down_weight.astype(jnp.bfloat16).T,
+            down_weight.astype(jnp.bfloat16),
         ),
-        (0, 0, 1, 0, 0),
-    )
-    down_scales = lax.all_gather(down_scale, "fs", axis=0, tiled=True)
-    outs = []
-    for tokens_here in tokens:
-        normed = norm_rows(tokens_here, mixer_gain).astype(jnp.bfloat16)
-        value = jnp.dot(normed, value_full, preferred_element_type=jnp.float32)
-        value = (value * value_scale.reshape(-1)).astype(jnp.bfloat16)
-        gating = jnp.dot(normed, gate_full, preferred_element_type=jnp.float32) * gate_scale.reshape(-1)
-        excess = pool_excess(value.reshape(1, seq_length, group_count, local_width)).astype(jnp.bfloat16)
-        both = swap(excess[0].reshape(seq_length, -1))
-        merged = []
-        for group in range(group_count):
-            cut = slice(group * local_width, (group + 1) * local_width)
-            pooled = jnp.dot(
-                jnp.concatenate([both[i][:, cut] for i in range(shares)], axis=1),
-                pool_full[group],
-                preferred_element_type=jnp.float32,
-            )
-            merged.append((jax.nn.sigmoid(gating[:, cut]) * (pooled * pool_scale[group])).astype(jnp.bfloat16))
-        merged = swap(jnp.concatenate(merged, axis=1))
-        merged = jnp.concatenate(
-            [
-                merged[i][:, group * local_width : (group + 1) * local_width]
-                for group in range(group_count)
-                for i in range(shares)
-            ],
-            axis=1,
-        )
-        middle = tokens_here.astype(jnp.float32) + merged.astype(jnp.float32)
-        normed_two = norm_rows(middle, channel_gain).astype(jnp.bfloat16)
-        upward = jnp.dot(normed_two, up_full, preferred_element_type=jnp.float32) * up_scale
-        hidden = jnp.square(jax.nn.relu(upward)).astype(jnp.bfloat16)
-        part = (
-            lax.dot_general(hidden, down_full, (((1,), (1,)), ((), ())), preferred_element_type=jnp.float32)
-            * down_scales
-        ).astype(jnp.bfloat16)
-        theirs = lax.dynamic_slice_in_dim(part, (1 - member) * kept_rows, kept_rows, 0)
-        mine = lax.dynamic_slice_in_dim(part, member * kept_rows, kept_rows, 0)
-        got = lax.ppermute(theirs, "tp", [(0, 1), (1, 0)])
-        summed = mine.astype(jnp.float32) + got.astype(jnp.float32)
-        own = lax.dynamic_slice_in_dim(middle, member * kept_rows, kept_rows, 0)
-        outs.append((own + summed).astype(jnp.bfloat16))
-    return jnp.stack(outs)
+    )
+    return out[None]
 
 
 def solution(mesh):
     sizes = dict(mesh.shape)
-    paired = sizes["rep"] == 2 and sizes["tp"] == 2 and sizes["fs"] % NY == 0 and sizes["fs"] <= 16
+    paired = sizes["rep"] == 2 and sizes["tp"] == 2 and sizes["fs"] % NY == 0 and sizes["fs"] == 8
+
+    def body(tokens, *rest):
+        value_scale, down_scale = rest[2], rest[-1]
+        if paired and tokens.shape[0] == 1 and value_scale.shape[1] == down_scale.shape[0]:
+            return paired_device(sizes, tokens, *rest)
+        return per_device(tokens, *rest)
+
     return jax.shard_map(
-        functools.partial(paired_device, sizes) if paired else per_device,
+        body,
         mesh=mesh,
         in_specs=(
             P(("rep", "fs"), None, None),

time: 341 us -> 220 us (0.65)
  waiting for transfers between devices: 82.4 us -> 0 us
  Pallas kernels: 154 us -> 204 us
  matrix products: 35.7 us -> 0 us
  other arithmetic: 31 us -> 5.39 us
  blocking collectives: 17.7 us -> 0 us
  local copies, waits for them, and re-layouts: 14.6 us -> 9.74 us
  starting transfers between devices: 4.51 us -> 0 us
    ppermute x3 -> x0, waiting for transfers between devices: 82.4 us -> none  [the longest x2 48 us: swap(): other = lax.ppermute(values, 'tp', [(0, 1), (1, 0)])]
    pallas_call x1, Pallas kernels: 154 us -> 204 us  [run_layer(): pl.pallas_call(functools.partial(layer_kernel, sizes), out_shape=jax.Shap...]
    dot_general x7 -> x0, matrix products: 35.7 us -> none  [the longest x1 21.5 us: paired_device(): lax.dot_general(hidden, down_full, (((1,), (1,)), ((), ())), preferred_el...]
    all_gather x1 -> x0, blocking collectives: 17.7 us -> none  [paired_device(): down_scales = lax.all_gather(down_scale, 'fs', axis=0, tiled=True)]
    another operation x3 -> x0, other arithmetic: 15.5 us -> none
    add x4 -> x0, other arithmetic: 5.33 us -> none  [the longest x1 3.7 us: paired_device(): middle = tokens_here.astype(jnp.float32) + merged.astype(jnp.float32)]
    select_n x2 -> x0, other arithmetic: 4.52 us -> none  [the longest x1 2.43 us: swap(): jnp.where(first, other, values)]
    ppermute x3 -> x0, starting transfers between devices: 4.51 us -> none  [the longest x2 3 us: swap(): other = lax.ppermute(values, 'tp', [(0, 1), (1, 0)])]
  transfers between devices with their start and end apart: 3 -> 0, of which waited for: 3 -> 0; matrix products, arithmetic and copies ran while one was open for 2% -> 0% of each run, Pallas kernels for 0% -> 0%
where the time goes in v2:
time: 220 us
  Pallas kernels  204 us (93%)
  local copies, waits for them, and re-layouts  9.74 us (4%)
  other arithmetic  5.39 us (2%)
    pallas_call x1, Pallas kernels, run_layer(): pl.pallas_call(functools.partial(layer_kernel, sizes), out_shape=jax.Shap...  204 us
    unnamed x12, local copies, waits for them, and re-layouts  8.47 us

profile of v2, /device:TPU:0, one launch (start us, length us, event | category | flops | bytes accessed | tf_op | source)
XLA Modules:
  0.0 219.5 jit_solution(12663437025997144989)
XLA Ops:
  0.0 0.0 copy-start.2
  0.0 1.4 copy.14
  1.4 1.3 copy.15
  2.6 1.3 copy.16
  3.9 1.3 broadcast_in_dim.8.refs_10_
  5.2 1.6 convert_element_type.17.refs_9_
  6.8 1.4 convert_element_type.15
  8.2 0.0 copy-start
  8.2 0.9 copy.17
  9.2 0.0 copy-done.2
  9.2 0.2 convert_element_type.16
  9.3 0.0 copy-start.1
  9.4 0.9 copy.18
  10.2 0.0 copy-done
  10.2 1.1 convert_element_type.18.refs_11_
  11.4 0.0 copy-done.1
  11.4 1.1 convert_element_type.19.refs_12_
  12.4 204.4 %shard_map.127 = bf16[384,2048]{1,0:T(8,128)(2,1)} custom-call(bf16[768,2048]{1,0:T(8,128)(2,1)} %bitcast.19, f32[1,2048]{1,0:T(1,128)} %bitcast.27, f32[1,1024]{1,0:T(1,128)} %bitcast.24, f32[1,1024]{1,0:T(1,128)} %bitcast.25, f32[1,1024]{1,0:T(1,128)} %bitcast.26, f32[1,2048]{1,0:T(1,128)} %bitcast.28, f32[1,2048]{1,0:T(1,128)} %bitcast.29, ...), custom_call_target="tpu_custom_call" | custom-call | tf_op jit(solution)/shard_map/pallas_call | solution.py:333
  216.8 2.7 %copy.20 = bf16[1,384,2048]{2,1,0:T(8,128)(2,1)} copy(bf16[1,384,2048]{2,1,0:T(8,128)(2,1)} %bitcast.18) | data formatting | bytes 3145728
Async XLA Ops:
  0.0 9.2 %copy-start.2 = (f32[256,4,256]{2,1,0:T(4,128)S(1)}, f32[256,4,256]{2,1,0:T(4,128)}, u32[]{:S(2)}) copy-start(f32[256,4,256]{2,1,0:T(4,128)} %param.17) | copy-start | bytes 3145732
  8.2 2.0 copy-start
  9.3 2.0 copy-start.1

commit v3 on v2

--- a/solution.py
+++ b/solution.py
@@ -103,6 +103,13 @@
         @pl.loop(0, self.nf)
         def _(k):
             pl.when(k != self.place)(lambda: self.copy(w, k, SIBLING, half=1 - self.rep).wait_recv())
+
+    def nearest(self, i):
+        ends = self.nz - 1 - self.z
+        short = jnp.minimum(self.z, ends)
+        near = self.z - (i + 1) // 2 if i % 2 else self.z + i // 2
+        far = jnp.where(self.z < ends, self.z + (i - short), self.z - (i - short))
+        return jnp.where(i <= 2 * short, near, far)
 
     def drain(self):
         for w in range(len(self.srcs)):
@@ -163,7 +170,7 @@
 
     def value_piece(group):
         cut = pl.ds(group * local, local)
-        value = jnp.dot(normed[...], fulls[VALUE][:, cut], preferred_element_type=jnp.float32) * value_scale[:, cut]
+        value = jnp.dot(normed[...], fulls[VALUE][:, cut], preferred_element_type=jnp.float32) * value_scale[group : group + 1]
         floats = value.astype(jnp.bfloat16).astype(jnp.float32)
         place = lax.broadcasted_iota(jnp.int32, floats.shape, 0)
         running = floats
@@ -181,7 +188,7 @@
         def _(i):
             at = pl.ds(pl.multiple_of(i * half, half), half)
             value = jnp.dot(normed[at, :], fulls[GATE][:, cut], preferred_element_type=jnp.float32)
-            gate[group, at, :] = jax.nn.sigmoid(value * gate_scale[:, cut])
+            gate[group, at, :] = jax.nn.sigmoid(value * gate_scale[group : group + 1])
 
     def pool_piece(group):
         excess_copy(group).wait_recv()
@@ -191,7 +198,7 @@
         pooled = jnp.dot(excess[group], mine, preferred_element_type=jnp.float32) + jnp.dot(
             excess_in[group], theirs, preferred_element_type=jnp.float32
         )
-        scale = pool_scale[:, pl.ds(group * local, local)]
+        scale = pool_scale[group : group + 1]
         merged[group] = (gate[group] * (pooled * scale)).astype(jnp.bfloat16)
         merged_copy(group).start()
 
@@ -234,24 +241,20 @@
         part = jnp.dot(hidden[at, :], weight, preferred_element_type=jnp.float32) * scale
         return part.astype(jnp.bfloat16)
 
+    def down_step(i, y):
+        k = g.nearest(i) * NY + y
+        if i or y is not g.y:
+            g.copy(SHOW, k, SIBLING, half=1 - g.rep).wait_recv()
+        part_out[k] = down_piece(k, (1 - member) * half)
+        part_copy(k).start()
+        part_own[k] = down_piece(k, member * half)
+
     def finish():
         wide = fulls[SHOW].shape[1]
-
-        @pl.loop(0, g.nf)
-        def _(k):
-            part_out[k] = down_piece(k, (1 - member) * half)
-            part_copy(k).start()
-
-        @pl.loop(0, g.nf)
-        def _(k):
-            part_own[k] = down_piece(k, member * half)
 
         @pl.loop(0, g.nf)
         def _(k):
             part_copy(k).wait_recv()
-
-        @pl.loop(0, g.nf)
-        def _(k):
             cut = pl.ds(pl.multiple_of(k * wide, wide), wide)
             summed = part_own[k].astype(jnp.float32) + part_in[k].astype(jnp.float32)
             out[:, cut] = (middle_of(k) + summed).astype(out.dtype)
@@ -282,6 +285,7 @@
         elif w == HIDE:
             work.extend(functools.partial(up_piece, i) for i in range(inner // local))
 
+    other = 1 - g.y
     for w in range(count):
         g.local(w).start()
     g.barrier((partner,))
@@ -298,14 +302,22 @@
                 if w:
                     g.across(w - 1, g.nz - 1)
                     queue(w - 1)
+                    if w == SHOW:
+                        work.append(functools.partial(down_step, 0, g.y))
             else:
                 g.across(w, d - 2)
-            emit(2)
+            if w == SHOW:
+                work.append(functools.partial(down_step, d, g.y))
+                if d > 1:
+                    work.append(functools.partial(down_step, d - 2, other))
+            emit(4 if w == SHOW else 2)
         g.across(w, g.nz - 2)
-        emit(2)
+        if w == SHOW:
+            work.append(functools.partial(down_step, g.nz - 2, other))
+        emit(4 if w == SHOW else 2)
+    emit(len(work))
     g.across(count - 1, g.nz - 1)
-    emit(len(work))
-    g.ready(count - 1)
+    down_step(g.nz - 1, other)
     finish()
     for group in range(groups):
         excess_copy(group).wait_send()
@@ -480,9 +492,9 @@
         tokens[0],
         (
             row(mixer_gain),
-            row(value_scale),
-            row(gate_scale),
-            row(pool_scale),
+            value_scale,
+            gate_scale,
+            pool_scale,
             row(channel_gain),
             row(up_scale),
         ),

time: 220 us -> 203 us (0.923)
  Pallas kernels: 204 us -> 191 us
  local copies, waits for them, and re-layouts: 9.74 us -> 5.9 us
    pallas_call x1, Pallas kernels: 204 us -> 191 us  [run_layer(): pl.pallas_call(functools.partial(layer_kernel, sizes), out_shape=jax.Shap...]
    unnamed x12 -> x9, local copies, waits for them, and re-layouts: 8.47 us -> 4.54 us
where the time goes in v3:
time: 203 us
  Pallas kernels  191 us (94%)
  local copies, waits for them, and re-layouts  5.9 us (3%)
  other arithmetic  5.39 us (3%)
    pallas_call x1, Pallas kernels, run_layer(): pl.pallas_call(functools.partial(layer_kernel, sizes), out_shape=jax.Shap...  191 us
    unnamed x9, local copies, waits for them, and re-layouts  4.54 us

profile of v3, /device:TPU:0, one launch (start us, length us, event | category | flops | bytes accessed | tf_op | source)
XLA Modules:
  0.0 202.8 jit_solution(3157994565317437579)
XLA Ops:
  0.0 0.0 copy-start.2
  0.0 1.4 broadcast_in_dim.8.refs_10_
  1.4 1.6 convert_element_type.17.refs_9_
  3.0 1.4 convert_element_type.15
  4.4 0.0 copy-start
  4.4 0.9 copy.14
  5.3 0.0 copy-done.2
  5.3 0.2 convert_element_type.16
  5.5 0.0 copy-start.1
  5.5 0.9 copy.15
  6.4 0.0 copy-done
  6.4 1.1 convert_element_type.18.refs_11_
  7.5 0.0 copy-done.1
  7.5 1.1 convert_element_type.19.refs_12_
  8.6 191.4 %shard_map.127 = bf16[384,2048]{1,0:T(8,128)(2,1)} custom-call(bf16[768,2048]{1,0:T(8,128)(2,1)} %bitcast.10, f32[1,2048]{1,0:T(1,128)} %bitcast.15, f32[4,256]{1,0:T(4,128)} %refs_2_.1, f32[4,256]{1,0:T(4,128)} %refs_3_.1, f32[4,256]{1,0:T(4,128)} %refs_4_.1, f32[1,2048]{1,0:T(1,128)} %bitcast.16, f32[1,2048]{1,0:T(1,128)} %bitcast.17, ...), custom_call_target="tpu_custom_call" | custom-call | tf_op jit(solution)/shard_map/pallas_call | solution.py:345
  200.1 2.7 %copy.17 = bf16[1,384,2048]{2,1,0:T(8,128)(2,1)} copy(bf16[1,384,2048]{2,1,0:T(8,128)(2,1)} %bitcast.9) | data formatting | bytes 3145728
Async XLA Ops:
  0.0 5.3 %copy-start.2 = (f32[256,4,256]{2,1,0:T(4,128)S(1)}, f32[256,4,256]{2,1,0:T(4,128)}, u32[]{:S(2)}) copy-start(f32[256,4,256]{2,1,0:T(4,128)} %param.17) | copy-start | bytes 3145732
  4.4 2.0 copy-start
  5.5 2.0 copy-start.1
